TPU v7x, 32 devices: a whole 2x2x4 slice. The times are simulated.
32 devices in a mesh: sp: 8 (over z, x), tp: 4 (over y, core).
Axes of the slice: x: 2, y: 2, z: 4, core: 2. Of those that a mesh axis runs over, the one named last changes fastest.
Arguments:
- residual: bfloat16 [4096, 2048], P('sp'), may hold values from -6 to 6
- queries: bfloat16 [4096, 1024], P('sp', 'tp'), may hold values from -384 to 384
- key_pairs: bfloat16 [4096, 1024], P('sp', 'tp'), may hold values from -384 to 384
- values: bfloat16 [4096, 1024], P('sp', 'tp'), may hold values from -6 to 6
- lambdas: float32 [8], P('tp'), may hold values from 0.3 to 0.8
- head_gain: float32 [128], replicated, may hold values from 0.1 to 1.9
- w_out: bfloat16 [1024, 2048], replicated, may hold values from -0.1875 to 0.1875
- norm_gain: float32 [2048], replicated, may hold values from 0.1 to 1.9
- w_gate: bfloat16 [2048, 5632], P('sp', 'tp'), may hold values from -0.125 to 0.125
- w_up: bfloat16 [2048, 5632], P('sp', 'tp'), may hold values from -0.125 to 0.125
- w_down: bfloat16 [5632, 2048], P('tp', 'sp'), may hold values from -0.078125 to 0.078125
Outputs:
- layer_out: bfloat16 [4096, 2048], P(('sp', 'tp'))
All inputs are finite; a program needn't handle non-finite values.
Results may differ from a plain program's by a relative error of at most 0.018.
Values may be sent and summed in bfloat16 or wider, within the bound.
A program may use at most 128 MiB of HBM per device.

v0:
```python
import math
import jax
import jax.numpy as jnp
from jax import lax
from jax.sharding import PartitionSpec as P

HD = 64


def per_device(
    residual, queries, key_pairs, values, lambdas, head_gain, w_out, norm_gain, w_gate, w_up, w_down
):
    local_rows = queries.shape[0]
    heads_here = lambdas.shape[0]
    value_width = values.shape[1] // heads_here
    score_scale = HD ** (-0.5)
    query_view = queries.reshape(local_rows, heads_here, 2, HD)

    def update(carry, key_block, value_block):
        highest, totals, mixture = carry
        scores = (
            jnp.einsum("qhmd,khmd->hmqk", query_view, key_block, preferred_element_type=jnp.float32)
            * score_scale
        )
        new_high = jnp.maximum(highest, jnp.max(scores, axis=-1))
        shrink = jnp.exp(highest - new_high)
        weights = jnp.exp(scores - new_high[..., None])
        totals = totals * shrink + jnp.sum(weights, axis=-1)
        mixture = mixture * shrink[..., None] + jnp.einsum(
            "hmqk,khe->hmqe",
            weights.astype(jnp.bfloat16),
            value_block,
            preferred_element_type=jnp.float32,
        )
        return (new_high, totals, mixture)

    initial = (
        jnp.full((heads_here, 2, local_rows), -jnp.inf, jnp.float32),
        jnp.zeros((heads_here, 2, local_rows), jnp.float32),
        jnp.zeros((heads_here, 2, local_rows, value_width), jnp.float32),
    )
    key_piece = lax.all_gather(key_pairs, "sp", axis=0, tiled=True)
    value_piece = lax.all_gather(values, "sp", axis=0, tiled=True)
    length = key_piece.shape[0]
    span = math.gcd(length, 512)
    key_blocks = key_piece.reshape(length // span, span, heads_here, 2, HD)
    value_blocks = value_piece.reshape(length // span, span, heads_here, value_width)

    def advance(position, inner):
        return update(inner, key_blocks[position], value_blocks[position])

    highest, totals, mixture = lax.fori_loop(0, length // span, advance, initial)
    mixed = mixture / totals[..., None]
    differ = mixed[:, 0] - lambdas[:, None, None] * mixed[:, 1]
    normed_heads = (
        differ * lax.rsqrt(jnp.mean(differ * differ, axis=-1, keepdims=True) + 1e-05) * head_gain
    )
    heads_out = (
        jnp.transpose(normed_heads, (1, 0, 2))
        .reshape(local_rows, heads_here * value_width)
        .astype(jnp.bfloat16)
    )
    tp_index = lax.axis_index("tp")
    own_rows = local_rows // lax.axis_size("tp")
    own_begin = tp_index * own_rows
    w_mine = lax.dynamic_slice_in_dim(
        w_out, tp_index * heads_here * value_width, heads_here * value_width, 0
    )
    projected = lax.psum_scatter(
        jnp.dot(heads_out, w_mine, preferred_element_type=jnp.float32).astype(jnp.bfloat16),
        "tp",
        scatter_dimension=0,
        tiled=True,
    ).astype(jnp.float32)
    residual_own = lax.dynamic_slice_in_dim(residual, own_begin, own_rows, 0)
    hidden_own = (residual_own.astype(jnp.float32) + projected).astype(jnp.bfloat16)
    stream_f = hidden_own.astype(jnp.float32)
    scaled = stream_f * lax.rsqrt(jnp.mean(stream_f * stream_f, axis=-1, keepdims=True) + 1e-05)
    normed_rows = lax.all_gather(
        (scaled * norm_gain).astype(jnp.bfloat16), "tp", axis=0, tiled=True
    )
    unit_width = w_gate.shape[1]
    joined = jnp.concatenate([w_gate, w_up], axis=1)
    both_sums = jnp.dot(
        normed_rows,
        lax.all_gather(joined, "sp", axis=0, tiled=True),
        preferred_element_type=jnp.float32,
    )
    gate_sum = both_sums[:, :unit_width]
    up_sum = both_sums[:, unit_width:]
    hidden_units = (jax.nn.silu(gate_sum) * up_sum).astype(jnp.bfloat16)
    down_whole = lax.all_gather(w_down, "sp", axis=1, tiled=True)
    ffn_out = lax.psum_scatter(
        jnp.dot(hidden_units, down_whole, preferred_element_type=jnp.float32).astype(jnp.bfloat16),
        "tp",
        scatter_dimension=0,
        tiled=True,
    ).astype(jnp.float32)
    return (hidden_own.astype(jnp.float32) + ffn_out).astype(jnp.bfloat16)


def solution(mesh):
    placed = (
        P("sp", None),
        P("sp", "tp"),
        P("sp", "tp"),
        P("sp", "tp"),
        P("tp"),
        P(),
        P(),
        P(),
        P("sp", "tp"),
        P("sp", "tp"),
        P("tp", "sp"),
    )
    return jax.shard_map(
        per_device, mesh=mesh, in_specs=placed, out_specs=P(("sp", "tp"), None), check_vma=False
    )
```

profile of v0, /device:TPU:0, one launch (start us, length us, event | category | flops | bytes accessed | tf_op | source)
XLA Modules:
  0.0 547.7 jit_solution(14696506700024109413)
XLA Ops:
  9.2 52.1 %all-gather.6.cloned.1.call-done = bf16[4096,256]{1,0:T(8,128)(2,1)} async-done(((bf16[512,256]{1,0:T(8,128)(2,1)}), bf16[4096,256]{1,0:T(8,128)(2,1)}) %all-gather.6.cloned.1.call-update) | async-done | bytes 2097168 | tf_op jit(solution)/shard_map/all_gather | solution.py:42
  61.3 8.3 %reshape.37 = bf16[8,512,2,2,64]{4,3,2,1,0:T(2,128)(2,1)} reshape(bf16[4096,256]{1,0:T(8,128)(2,1)} %all-gather.6.cloned.1.call-done) | data formatting | bytes 4194304 | tf_op jit(solution)/shard_map/reshape | solution.py:46
  69.6 9.1 %copy.19 = bf16[8,512,2,2,64]{1,4,3,2,0:T(8,128)(2,1)S(1)} copy(bf16[8,512,2,2,64]{4,3,2,1,0:T(2,128)(2,1)} %reshape.37) | data formatting | bytes 4194304
  78.7 32.4 %all-gather.8.cloned.1.call-done = bf16[4096,256]{1,0:T(8,128)(2,1)} async-done(((bf16[512,256]{1,0:T(8,128)(2,1)}), bf16[4096,256]{1,0:T(8,128)(2,1)}) %all-gather.8.cloned.1.call-update) | async-done | bytes 2097168 | tf_op jit(solution)/shard_map/all_gather | solution.py:43
  111.1 4.0 reshape.38
  115.0 67.2 %while.18 = (s32[]{:T(128)}, f32[2,2,512]{2,1,0:T(2,128)S(1)}, f32[2,2,512]{2,1,0:T(2,128)S(1)}, f32[2,2,512,128]{3,2,1,0:T(8,128)S(1)}, bf16[8,512,2,2,64]{1,4,...) while((s32[]{:T(128)}, f32[2,2,512]{2,1,0:T(2,128)S(1)}, ...), condition=%wide.region_3.0_spmd.clone, body=%wide.region_0.0_spmd.clone.sunk | while | flops 411838464 | bytes 32899212 | solution.py:52
  115.0 2.7 bitcast_reduce_fusion.2
  117.7 3.0 fusion.44
  120.8 1.1 constant_dynamic-slice_fusion.2
  122.0 1.4 fusion.46
  123.4 2.7 bitcast_reduce_fusion.2
  126.1 3.0 fusion.44
  129.2 1.1 constant_dynamic-slice_fusion.2
  130.4 1.4 fusion.46
  131.8 2.7 bitcast_reduce_fusion.2
  134.5 3.0 fusion.44
  138.8 1.4 fusion.46
  140.2 2.7 bitcast_reduce_fusion.2
  142.9 3.0 fusion.44
  146.0 1.1 constant_dynamic-slice_fusion.2
  147.2 1.4 fusion.46
  148.6 2.7 bitcast_reduce_fusion.2
  151.3 3.0 fusion.44
  154.4 1.1 constant_dynamic-slice_fusion.2
  155.6 1.4 fusion.46
  157.0 2.7 bitcast_reduce_fusion.2
  159.7 3.0 fusion.44
  162.8 1.1 constant_dynamic-slice_fusion.2
  164.0 1.4 fusion.46
  165.4 2.7 bitcast_reduce_fusion.2
  168.1 3.0 fusion.44
  171.2 1.1 constant_dynamic-slice_fusion.2
  172.4 1.4 fusion.46
  173.8 2.7 bitcast_reduce_fusion.2
  176.5 3.0 fusion.44
  179.6 1.1 constant_dynamic-slice_fusion.2
  180.8 1.4 fusion.46
  183.2 3.3 convolution_convert_fusion
  186.6 29.8 %reduce-scatter.3.cloned.1.call-done = bf16[128,2048]{1,0:T(8,128)(2,1)} async-done(((bf16[512,2048]{1,0:T(8,128)(2,1)}), bf16[128,2048]{1,0:T(8,128)(2,1)}) %reduce-scatter.3.cloned.1.call-update) | async-done | bytes 524304 | tf_op jit(solution)/shard_map/reduce_scatter | solution.py:69
  216.4 1.5 fusion.20
  219.0 1.2 pad_maximum_fusion
  221.0 20.6 %all-gather.10.cloned.1.call-done = bf16[512,2048]{1,0:T(8,128)(2,1)} async-done(((bf16[128,2048]{1,0:T(8,128)(2,1)}), bf16[512,2048]{1,0:T(8,128)(2,1)}) %all-gather.10.cloned.1.call-update) | async-done | bytes 2097168 | tf_op jit(solution)/shard_map/all_gather | solution.py:79
  241.6 165.4 %all-gather.12.cloned.1.call-done = bf16[2048,2816]{1,0:T(8,128)(2,1)} async-done(((bf16[256,2816]{1,0:T(8,128)(2,1)}), bf16[2048,2816]{1,0:T(8,128)(2,1)}) %all-gather.12.cloned.1.call-update) | async-done | bytes 11534352 | tf_op jit(solution)/shard_map/all_gather | solution.py:86
  407.0 12.5 %fusion.29 = f32[512,2816]{1,0:T(8,128)} fusion(bf16[512,2048]{1,0:T(8,128)(2,1)} %all-gather.10.cloned.1.call-done, bf16[2048,2816]{1,0:T(8,128)(2,1)} %all-gather.12.cloned.1.call-done), kind=kOutput, calls=%fused_computation.48 | convolution fusion | flops 5905580032 | bytes 19398656 | tf_op jit(solution)/shard_map/dot_general | solution.py:84
  419.5 80.7 %all-gather.14.cloned.1.call-done = bf16[1408,2048]{1,0:T(8,128)(2,1)} async-done(((bf16[1408,256]{1,0:T(8,128)(2,1)}), bf16[1408,2048]{1,0:T(8,128)(2,1)}) %all-gather.14.cloned.1.call-update) | async-done | bytes 5767184 | tf_op jit(solution)/shard_map/all_gather | solution.py:92
  500.2 9.1 %convolution_convert_fusion.1 = bf16[512,2048]{1,0:T(8,128)(2,1)} fusion(bf16[1408,2048]{1,0:T(8,128)(2,1)} %all-gather.14.cloned.1.call-done, f32[512,2816]{1,0:T(8,128)} %fusion.29), kind=kOutput, calls=%fused_computation.23 | convolution fusion | flops 2958163968 | bytes 13631488 | tf_op jit(solution)/shard_map/dot_general | solution.py:94
  509.4 29.5 %reduce-scatter.5.cloned.1.call-done = bf16[128,2048]{1,0:T(8,128)(2,1)} async-done(((bf16[512,2048]{1,0:T(8,128)(2,1)}), bf16[128,2048]{1,0:T(8,128)(2,1)}) %reduce-scatter.5.cloned.1.call-update) | async-done | bytes 524304 | tf_op jit(solution)/shard_map/reduce_scatter | solution.py:93
  538.9 2.0 fusion.23
  (77 shorter events, 6.9 us)
Async XLA Ops:
  6.5 54.8 %all-gather.6.cloned.1.call-start = ((), (), s32[]{:S(2)}) async-start(), calls=%async_computation.2 | async-start | bytes 2359296 | tf_op jit(solution)/shard_map/all_gather | solution.py:42
  7.3 103.8 %all-gather.8.cloned.1.call-start = ((), (), s32[]{:S(2)}) async-start(), calls=%async_computation.3 | async-start | bytes 2359296 | tf_op jit(solution)/shard_map/all_gather | solution.py:43
  8.0 208.4 %reduce-scatter.3.cloned.1.call-start = ((), (), s32[]{:S(2)}) async-start(), calls=%async_computation.4 | async-start | bytes 2621440 | tf_op jit(solution)/shard_map/reduce_scatter | solution.py:69
  117.7 4.2 copy-start
  126.1 4.2 copy-start
  134.5 4.2 copy-start
  142.9 4.2 copy-start
  151.3 4.2 copy-start
  159.7 4.2 copy-start
  168.1 4.2 copy-start
  176.5 4.2 copy-start
  182.2 0.7 copy-start.4
  182.2 0.8 copy-start.5
  186.5 31.4 %copy-start.3 = (f32[2048]{0:T(1024)S(1)}, f32[2048]{0:T(1024)}, u32[]{:S(2)}) copy-start(f32[2048]{0:T(1024)} %param.20) | copy-start | bytes 24580
  186.5 32.4 %copy-start.1 = (bf16[256,1408]{1,0:T(8,128)(2,1)S(1)}, bf16[256,1408]{1,0:T(8,128)(2,1)}, u32[]{:S(2)}) copy-start(bf16[256,1408]{1,0:T(8,128)(2,1)} %param.22) | copy-start | bytes 2162692
  186.5 32.4 %copy-start.2 = (bf16[256,1408]{1,0:T(8,128)(2,1)S(1)}, bf16[256,1408]{1,0:T(8,128)(2,1)}, u32[]{:S(2)}) copy-start(bf16[256,1408]{1,0:T(8,128)(2,1)} %param.21) | copy-start | bytes 2162692
  186.6 55.1 %all-gather.10.cloned.1.call-start = ((), (), s32[]{:S(2)}) async-start(), calls=%async_computation.5 | async-start | bytes 2621440 | tf_op jit(solution)/shard_map/all_gather | solution.py:79
  218.9 188.1 %all-gather.12.cloned.1.call-start = ((), (), s32[]{:S(2)}) async-start(), calls=%async_computation.6 | async-start | bytes 12976128 | tf_op jit(solution)/shard_map/all_gather | solution.py:86
  220.2 280.0 %all-gather.14.cloned.1.call-start = ((), (), s32[]{:S(2)}) async-start(), calls=%async_computation.7 | async-start | bytes 6488064 | tf_op jit(solution)/shard_map/all_gather | solution.py:92
  220.8 318.1 %reduce-scatter.5.cloned.1.call-start = ((), (), s32[]{:S(2)}) async-start(), calls=%async_computation.8 | async-start | bytes 2621440 | tf_op jit(solution)/shard_map/reduce_scatter | solution.py:93
Sparse Core Ops, SparseCore 0:
  9.5 51.7 all-gather.5
  63.4 47.6 all-gather.7
  186.7 29.6 reduce-scatter.2
  219.0 22.5 all-gather.9
  243.7 163.2 all-gather.11
  408.9 91.2 all-gather.13
  509.5 29.3 reduce-scatter.4
where the time goes:
time: 548 us
  waiting for transfers between devices  412 us (75%)
  matrix products  57.9 us (11%)
  local copies, waits for them, and re-layouts  32.1 us (6%)
  other arithmetic  30.8 us (6%)
  between operations  13.6 us (2%)
    all_gather x1, waiting for transfers between devices, per_device(): lax.all_gather(joined, 'sp', axis=0, tiled=True)  165 us
    all_gather x1, waiting for transfers between devices, per_device(): down_whole = lax.all_gather(w_down, 'sp', axis=1, tiled=True)  80.7 us
    all_gather x1, waiting for transfers between devices, per_device(): key_piece = lax.all_gather(key_pairs, 'sp', axis=0, tiled=True)  52.1 us
    all_gather x1, waiting for transfers between devices, per_device(): value_piece = lax.all_gather(values, 'sp', axis=0, tiled=True)  32.4 us
    reduce_scatter x1, waiting for transfers between devices, per_device(): lax.psum_scatter(jnp.dot(heads_out, w_mine, preferred_element_type=jnp.fl...  29.8 us
    reduce_scatter x1, waiting for transfers between devices, per_device(): lax.psum_scatter(jnp.dot(hidden_units, down_whole, preferred_element_type...  29.5 us
    reduce_sum x8, other arithmetic, update(): totals = totals * shrink + jnp.sum(weights, axis=-1)  24.3 us
    dot_general x8, matrix products, update(): jnp.einsum('qhmd,khmd->hmqk', query_view, key_block, preferred_element_ty...  21.7 us
  transfers between devices with their start and end apart: 7, of which 7 were waited for; matrix products, arithmetic and copies ran while one was open for 6% of the time, Pallas kernels for 0%

commit v1 on v0

--- a/solution.py
+++ b/solution.py
@@ -89,7 +89,8 @@
     gate_sum = both_sums[:, :unit_width]
     up_sum = both_sums[:, unit_width:]
     hidden_units = (jax.nn.silu(gate_sum) * up_sum).astype(jnp.bfloat16)
-    down_whole = lax.all_gather(w_down, "sp", axis=1, tiled=True)
+    now = jax.lax.all_gather(w_down, "sp")
+    down_whole = jnp.concatenate(now, axis=1)
     ffn_out = lax.psum_scatter(
         jnp.dot(hidden_units, down_whole, preferred_element_type=jnp.float32).astype(jnp.bfloat16),
         "tp",

time: 548 us -> 553 us (level)
  local copies, waits for them, and re-layouts: 32.1 us -> 40.4 us
  matrix products: 57.9 us -> 51.2 us
    all_gather x1, waiting for transfers between devices: 80.7 us -> 90.5 us  [per_device(): now = jax.lax.all_gather(w_down, 'sp')]
    reshape x0 -> x1, local copies, waits for them, and re-layouts: none -> 8.27 us  [per_device(): down_whole = jnp.concatenate(now, axis=1)]
    all_gather x1, waiting for transfers between devices: 20.6 us -> 13.9 us  [per_device(): lax.all_gather((scaled * norm_gain).astype(jnp.bfloat16), 'tp', axis=0, t...]
where the time goes in v1:
time: 553 us; the launch traced here: 552 us
  waiting for transfers between devices  415 us (75%)
  matrix products  51.2 us (9%)
  local copies, waits for them, and re-layouts  40.4 us (7%)
  other arithmetic  30.8 us (6%)
  between operations  13.6 us (2%)
    all_gather x1, waiting for transfers between devices, per_device(): lax.all_gather(joined, 'sp', axis=0, tiled=True)  165 us
    all_gather x1, waiting for transfers between devices, per_device(): now = jax.lax.all_gather(w_down, 'sp')  90.5 us
    all_gather x1, waiting for transfers between devices, per_device(): key_piece = lax.all_gather(key_pairs, 'sp', axis=0, tiled=True)  52.1 us
    all_gather x1, waiting for transfers between devices, per_device(): value_piece = lax.all_gather(values, 'sp', axis=0, tiled=True)  32.4 us
    reduce_scatter x1, waiting for transfers between devices, per_device(): lax.psum_scatter(jnp.dot(hidden_units, down_whole, preferred_element_type...  29.5 us
    reduce_scatter x1, waiting for transfers between devices, per_device(): lax.psum_scatter(jnp.dot(heads_out, w_mine, preferred_element_type=jnp.fl...  29.2 us
    reduce_sum x8, other arithmetic, update(): totals = totals * shrink + jnp.sum(weights, axis=-1)  24.3 us
    dot_general x8, matrix products, update(): jnp.einsum('qhmd,khmd->hmqk', query_view, key_block, preferred_element_ty...  21.7 us
  transfers between devices with their start and end apart: 7, of which 7 were waited for; matrix products, arithmetic and copies ran while one was open for 6% of the time, Pallas kernels for 0%

profile of v1, /device:TPU:0, one launch (start us, length us, event | category | flops | bytes accessed | tf_op | source)
XLA Modules:
  0.0 551.6 jit_solution(15107782710235911323)
XLA Ops:
  9.2 52.1 %all-gather.7.cloned.1.call-done = bf16[4096,256]{1,0:T(8,128)(2,1)} async-done(((bf16[512,256]{1,0:T(8,128)(2,1)}), bf16[4096,256]{1,0:T(8,128)(2,1)}) %all-gather.7.cloned.1.call-update) | async-done | bytes 2097168 | tf_op jit(solution)/shard_map/all_gather | solution.py:42
  61.3 8.3 %reshape.46 = bf16[8,512,2,2,64]{4,3,2,1,0:T(2,128)(2,1)} reshape(bf16[4096,256]{1,0:T(8,128)(2,1)} %all-gather.7.cloned.1.call-done) | data formatting | bytes 4194304 | tf_op jit(solution)/shard_map/reshape | solution.py:46
  69.6 9.1 %copy.27 = bf16[8,512,2,2,64]{1,4,3,2,0:T(8,128)(2,1)S(1)} copy(bf16[8,512,2,2,64]{4,3,2,1,0:T(2,128)(2,1)} %reshape.46) | data formatting | bytes 4194304
  78.7 32.4 %all-gather.9.cloned.1.call-done = bf16[4096,256]{1,0:T(8,128)(2,1)} async-done(((bf16[512,256]{1,0:T(8,128)(2,1)}), bf16[4096,256]{1,0:T(8,128)(2,1)}) %all-gather.9.cloned.1.call-update) | async-done | bytes 2097168 | tf_op jit(solution)/shard_map/all_gather | solution.py:43
  111.1 4.0 reshape.47
  115.1 67.1 %while.18 = (s32[]{:T(128)}, f32[2,2,512]{2,1,0:T(2,128)S(1)}, f32[2,2,512]{2,1,0:T(2,128)S(1)}, f32[2,2,512,128]{3,2,1,0:T(8,128)S(1)}, bf16[8,512,2,2,64]{1,4,...) while((s32[]{:T(128)}, f32[2,2,512]{2,1,0:T(2,128)S(1)}, ...), condition=%wide.region_3.0_spmd.clone, body=%wide.region_0.0_spmd.clone.sunk | while | flops 411838464 | bytes 32899212 | solution.py:52
  115.1 2.7 bitcast_reduce_fusion.2
  117.8 3.0 fusion.44
  120.9 1.1 constant_dynamic-slice_fusion.2
  122.0 1.4 fusion.46
  123.4 2.7 bitcast_reduce_fusion.2
  126.2 3.0 fusion.44
  129.2 1.1 constant_dynamic-slice_fusion.2
  130.4 1.4 fusion.46
  131.8 2.7 bitcast_reduce_fusion.2
  134.6 3.0 fusion.44
  137.6 1.1 constant_dynamic-slice_fusion.2
  138.8 1.4 fusion.46
  140.2 2.7 bitcast_reduce_fusion.2
  143.0 3.0 fusion.44
  147.2 1.4 fusion.46
  148.6 2.7 bitcast_reduce_fusion.2
  151.3 3.0 fusion.44
  154.4 1.1 constant_dynamic-slice_fusion.2
  155.6 1.4 fusion.46
  157.0 2.7 bitcast_reduce_fusion.2
  159.7 3.0 fusion.44
  164.0 1.4 fusion.46
  165.4 2.7 bitcast_reduce_fusion.2
  168.1 3.0 fusion.44
  171.2 1.1 constant_dynamic-slice_fusion.2
  172.4 1.4 fusion.46
  173.8 2.7 bitcast_reduce_fusion.2
  176.5 3.0 fusion.44
  179.6 1.1 constant_dynamic-slice_fusion.2
  180.7 1.4 fusion.46
  183.2 3.3 convolution_convert_fusion
  187.2 29.2 %reduce-scatter.3.cloned.1.call-done = bf16[128,2048]{1,0:T(8,128)(2,1)} async-done(((bf16[512,2048]{1,0:T(8,128)(2,1)}), bf16[128,2048]{1,0:T(8,128)(2,1)}) %reduce-scatter.3.cloned.1.call-update) | async-done | bytes 524304 | tf_op jit(solution)/shard_map/reduce_scatter | solution.py:69
  216.4 1.5 fusion.20
  219.0 1.3 pad_maximum_fusion
  220.3 90.5 %all-gather.15.cloned.1.call-done = bf16[11264,256]{1,0:T(8,128)(2,1)} async-done(((bf16[1408,256]{1,0:T(8,128)(2,1)}), bf16[11264,256]{1,0:T(8,128)(2,1)}) %all-gather.15.cloned.1.call-update) | async-done | bytes 5767184 | tf_op jit(solution)/shard_map/all_gather | solution.py:92
  310.8 8.3 %copy.31 = bf16[1408,8,256]{0,2,1:T(8,128)(2,1)} copy(bf16[1408,8,256]{2,0,1:T(8,128)(2,1)} %bitcast.67) | data formatting | bytes 11534336 | tf_op jit(solution)/shard_map/reshape | solution.py:93
  319.0 13.9 %all-gather.11.cloned.1.call-done = bf16[512,2048]{1,0:T(8,128)(2,1)} async-done(((bf16[128,2048]{1,0:T(8,128)(2,1)}), bf16[512,2048]{1,0:T(8,128)(2,1)}) %all-gather.11.cloned.1.call-update) | async-done | bytes 2097168 | tf_op jit(solution)/shard_map/all_gather | solution.py:79
  333.0 165.4 %all-gather.13.cloned.1.call-done = bf16[2048,2816]{1,0:T(8,128)(2,1)} async-done(((bf16[256,2816]{1,0:T(8,128)(2,1)}), bf16[2048,2816]{1,0:T(8,128)(2,1)}) %all-gather.13.cloned.1.call-update) | async-done | bytes 11534352 | tf_op jit(solution)/shard_map/all_gather | solution.py:86
  498.3 10.3 %fusion.29 = f32[512,2816]{1,0:T(8,128)S(1)} fusion(bf16[512,2048]{1,0:T(8,128)(2,1)} %all-gather.11.cloned.1.call-done, bf16[2048,2816]{1,0:T(8,128)(2,1)} %all-gather.13.cloned.1.call-done), kind=kOutput, calls=%fused_computation.48 | convolution fusion | flops 5905580032 | bytes 19398656 | tf_op jit(solution)/shard_map/dot_general | solution.py:84
  508.6 4.7 convolution_convert_fusion.1
  513.4 29.5 %reduce-scatter.5.cloned.1.call-done = bf16[128,2048]{1,0:T(8,128)(2,1)} async-done(((bf16[512,2048]{1,0:T(8,128)(2,1)}), bf16[128,2048]{1,0:T(8,128)(2,1)}) %reduce-scatter.5.cloned.1.call-update) | async-done | bytes 524304 | tf_op jit(solution)/shard_map/reduce_scatter | solution.py:94
  542.8 2.0 fusion.23
  (80 shorter events, 7.9 us)
Async XLA Ops:
  6.5 54.8 %all-gather.7.cloned.1.call-start = ((), (), s32[]{:S(2)}) async-start(), calls=%async_computation.2 | async-start | bytes 2359296 | tf_op jit(solution)/shard_map/all_gather | solution.py:42
  7.3 103.8 %all-gather.9.cloned.1.call-start = ((), (), s32[]{:S(2)}) async-start(), calls=%async_computation.3 | async-start | bytes 2359296 | tf_op jit(solution)/shard_map/all_gather | solution.py:43
  8.0 208.4 %reduce-scatter.3.cloned.1.call-start = ((), (), s32[]{:S(2)}) async-start(), calls=%async_computation.4 | async-start | bytes 2621440 | tf_op jit(solution)/shard_map/reduce_scatter | solution.py:69
  117.8 4.2 copy-start
  126.2 4.2 copy-start
  134.5 4.2 copy-start
  142.9 4.2 copy-start
  151.3 4.2 copy-start
  159.7 4.2 copy-start
  168.1 4.2 copy-start
  176.5 4.2 copy-start
  182.2 0.7 copy-start.5
  182.2 0.8 copy-start.6
  186.5 31.4 %copy-start.4 = (f32[2048]{0:T(1024)S(1)}, f32[2048]{0:T(1024)}, u32[]{:S(2)}) copy-start(f32[2048]{0:T(1024)} %param.20) | copy-start | bytes 24580
  186.5 32.4 %copy-start.2 = (bf16[256,1408]{1,0:T(8,128)(2,1)S(1)}, bf16[256,1408]{1,0:T(8,128)(2,1)}, u32[]{:S(2)}) copy-start(bf16[256,1408]{1,0:T(8,128)(2,1)} %param.22) | copy-start | bytes 2162692
  186.5 32.4 %copy-start.3 = (bf16[256,1408]{1,0:T(8,128)(2,1)S(1)}, bf16[256,1408]{1,0:T(8,128)(2,1)}, u32[]{:S(2)}) copy-start(bf16[256,1408]{1,0:T(8,128)(2,1)} %param.21) | copy-start | bytes 2162692
  186.5 124.2 %all-gather.15.cloned.1.call-start = ((), (), s32[]{:S(2)}) async-start(), calls=%async_computation.8 | async-start | bytes 6488064 | tf_op jit(solution)/shard_map/all_gather | solution.py:92
  187.1 145.8 %all-gather.11.cloned.1.call-start = ((), (), s32[]{:S(2)}) async-start(), calls=%async_computation.5 | async-start | bytes 2621440 | tf_op jit(solution)/shard_map/all_gather | solution.py:79
  218.9 279.5 %all-gather.13.cloned.1.call-start = ((), (), s32[]{:S(2)}) async-start(), calls=%async_computation.6 | async-start | bytes 12976128 | tf_op jit(solution)/shard_map/all_gather | solution.py:86
  220.3 322.6 %reduce-scatter.5.cloned.1.call-start = ((), (), s32[]{:S(2)}) async-start(), calls=%async_computation.7 | async-start | bytes 2621440 | tf_op jit(solution)/shard_map/reduce_scatter | solution.py:94
  498.3 10.3 %copy-start.1 = (bf16[1408,8,256]{0,2,1:T(8,128)(2,1)S(1)}, bf16[1408,8,256]{0,2,1:T(8,128)(2,1)}, u32[]{:S(2)}) copy-start(bf16[1408,8,256]{0,2,1:T(8,128)(2,1)} %copy.31) | copy-start | bytes 17301508
Sparse Core Ops, SparseCore 0:
  9.5 51.7 all-gather.6
  63.4 47.6 all-gather.8
  186.7 29.6 reduce-scatter.2
  218.4 92.2 all-gather.14
  312.2 20.7 all-gather.10
  335.0 163.2 all-gather.12
  513.5 29.3 reduce-scatter.4
